TPU v7x, 128 devices: a whole 4x4x4 slice. The times are simulated.
128 devices in a mesh: sp: 32 (over z, y, core), tp: 4 (over x).
Axes of the slice: x: 4, y: 4, z: 4, core: 2. Of those that a mesh axis runs over, the one named last changes fastest.
Arguments:
- residual_in: bfloat16 [65536, 2048], P(('sp', 'tp')), may hold values from -6 to 6
- conv_input: bfloat16 [65536, 1024], P('sp', 'tp'), may hold values from -6 to 6
- input_gate: bfloat16 [65536, 1024], P('sp', 'tp'), may hold values from -6 to 6
- output_gate: bfloat16 [65536, 1024], P('sp', 'tp'), may hold values from -6 to 6
- conv_taps: bfloat16 [3, 1024], P(None, 'tp'), may hold values from -3.5 to 3.5
- doc_ids: int32 [65536], P('sp'), may hold values from 0 to 15, never falling along the last dimension, each value on 1 to 8192 neighbouring positions
- proj_weight: bfloat16 [1024, 2048], replicated, may hold values from -0.1875 to 0.1875
- norm_gain: float32 [2048], replicated, may hold values from 0.1 to 1.9
- expert_ids: int32 [65536, 2], P(('sp', 'tp')), may hold values from 0 to 31, all different within a row; in each aligned block of 512 rows (0 to 511, 512 to 1023, ...) at most 64 rows name the same one
- expert_weight: float32 [65536, 2], P(('sp', 'tp')), may hold values from 0.05 to 1
- w_gate: bfloat16 [32, 2048, 512], P('sp'), may hold values from -0.125 to 0.125
- w_up: bfloat16 [32, 2048, 512], P('sp'), may hold values from -0.125 to 0.125
- w_down: bfloat16 [32, 512, 2048], P('sp'), may hold values from -0.25 to 0.25
Outputs:
- layer_out: bfloat16 [65536, 2048], P(('sp', 'tp'))
Inputs may be any that keep to these rules, and one draw needn't show every extreme that they name: `doc_ids`: numbers never fall along the sequence; one document spans at most 8192 positions. `expert_ids`: a token's two experts differ; in each aligned block of rows that one device holds, no expert is named more than 64 times, a bound that some block reaches.
All inputs are finite; a program needn't handle non-finite values.
Results may differ from a plain program's by a relative error of at most 0.0047.
Values may be sent and summed in bfloat16 or wider, within the bound.
No kernel may reach another device: no remote copies, remote signals or barrier semaphores. Data moves between devices by JAX's collectives and lax.ppermute only.
A program may use at most 128 MiB of HBM per device.

v0:
```python
import jax
import jax.numpy as jnp
from jax import lax
from jax.sharding import PartitionSpec as P

EXPERTS = 32
CAP = 64


epsilon = 1e-06


def from_behind(x, axis, by):
    devices = lax.axis_size(axis)
    pairs = [(i, i + by) for i in range(devices) if 0 <= i + by < devices]
    return lax.ppermute(x, axis, pairs)


def per_device(
    residual_in,
    conv_input,
    input_gate,
    output_gate,
    conv_taps,
    doc_ids,
    proj_weight,
    norm_gain,
    expert_ids,
    expert_weight,
    w_gate,
    w_up,
    w_down,
):
    kernel_width = conv_taps.shape[0]
    rim_rows = kernel_width - 1
    product = input_gate.astype(jnp.float32) * conv_input.astype(jnp.float32)
    doc_float = doc_ids.astype(jnp.float32)
    prev_in, prev_ids = from_behind((product[-rim_rows:], doc_float[-rim_rows:]), "sp", 1)
    padded_in = jnp.concatenate([prev_in, product], axis=0)
    padded_ids = jnp.concatenate([prev_ids, doc_float], axis=0)
    length = product.shape[0]
    conv_sum = jnp.zeros(product.shape, jnp.float32)
    for offset in range(kernel_width):
        same_doc = padded_ids[offset : offset + length] == doc_float
        term = conv_taps[offset].astype(jnp.float32)[None, :] * padded_in[offset : offset + length]
        conv_sum = conv_sum + jnp.where(same_doc[:, None], term, 0.0)
    gated = (output_gate.astype(jnp.float32) * conv_sum).astype(jnp.bfloat16)
    regrouped = lax.all_to_all(gated, "tp", split_axis=0, concat_axis=1, tiled=True)
    mixed = jnp.dot(regrouped, proj_weight, preferred_element_type=jnp.float32)
    hidden = residual_in.astype(jnp.float32) + mixed
    scale_rows = lax.rsqrt(jnp.mean(hidden * hidden, axis=-1, keepdims=True) + epsilon)
    normed = (hidden * scale_rows * norm_gain[None, :]).astype(jnp.bfloat16)
    local_experts = w_gate.shape[0]
    model_width = normed.shape[1]
    flat_ids = expert_ids.reshape(-1)
    one_hot = (flat_ids[:, None] == jnp.arange(EXPERTS, dtype=jnp.int32)[None, :]).astype(jnp.int32)
    before = jnp.cumsum(one_hot, axis=0) - one_hot
    slot_index = flat_ids * CAP + jnp.sum(before * one_hot, axis=1)
    source_rows = jnp.repeat(normed, 2, axis=0)
    buffer = jnp.zeros((EXPERTS * CAP, model_width), jnp.bfloat16).at[slot_index].set(source_rows)
    buffer = buffer.reshape(lax.axis_size("sp"), local_experts, CAP, model_width)
    slots = lax.all_to_all(buffer, "sp", split_axis=0, concat_axis=0, tiled=True)
    gate_val = jnp.einsum("aend,edf->aenf", slots, w_gate, preferred_element_type=jnp.float32)
    up_val = jnp.einsum("aend,edf->aenf", slots, w_up, preferred_element_type=jnp.float32)
    act_rows = (jax.nn.silu(gate_val) * up_val).astype(jnp.bfloat16)
    expert_out = jnp.einsum(
        "aenf,efd->aend", act_rows, w_down, preferred_element_type=jnp.float32
    ).astype(jnp.bfloat16)
    returned = lax.all_to_all(expert_out, "sp", split_axis=0, concat_axis=0, tiled=True).reshape(
        EXPERTS * CAP, model_width
    )
    picked = returned[slot_index].astype(jnp.float32) * expert_weight.reshape(-1)[:, None]
    expert_sum = jnp.sum(picked.reshape(-1, 2, model_width), axis=1)
    return (hidden + expert_sum).astype(jnp.bfloat16)


def solution(mesh):
    return jax.shard_map(
        per_device,
        mesh=mesh,
        in_specs=(
            P(("sp", "tp"), None),
            P("sp", "tp"),
            P("sp", "tp"),
            P("sp", "tp"),
            P(None, "tp"),
            P("sp"),
            P(),
            P(),
            P(("sp", "tp"), None),
            P(("sp", "tp"), None),
            P("sp", None, None),
            P("sp", None, None),
            P("sp", None, None),
        ),
        out_specs=P(("sp", "tp"), None),
        check_vma=False,
    )
```

profile of v0, /device:TPU:0, one launch (start us, length us, event | category | flops | bytes accessed | tf_op | source)
XLA Modules:
  0.0 357.5 jit_solution(186289497554102982)
XLA Ops:
  0.0 0.0 copy-start
  0.0 0.0 copy-start.7
  0.0 0.0 copy-start.8
  0.0 0.0 copy-start.10
  0.0 0.8 convert_element_type.61
  0.9 0.1 slice.46
  0.9 1.3 collective-permute-start
  2.2 1.8 convert_multiply_fusion
  4.0 0.0 copy-start.4
  4.0 1.3 copy-done.4
  5.3 4.3 %collective-permute-start.1 = (f32[2,256]{1,0:T(2,128)S(1)}, f32[2,256]{1,0:T(2,128)S(1)}, u32[]{:S(2)}, u32[]{:S(2)}) collective-permute-start(f32[2,256]{1,0:T(2,128)S(1)} %slice.49), channel_id=1, source_target_pairs={{0,4},{4,8},{8,12},{12,16},{16,20},{20,24},{24,28},{28,32},{32,36}... | collective-permute-start | bytes 6152 | tf_op jit(solution)/shard_map/ppermute | solution.py:16
  9.7 0.0 copy-done.7
  9.7 0.0 copy-done.8
  9.7 0.1 copy.30
  9.8 0.2 eq.41
  10.0 0.8 eq.37
  10.8 0.0 copy-done.10
  10.8 9.0 %reduce-window.6 = s32[32,8,128]{2,1,0:T(8,128)S(1)} reduce-window(s32[32,8,128]{2,1,0:T(8,128)S(1)} %fusion.36, s32[]{:T(128)} %constant.6.clone.1), window={size=1x1x128 pad=0_0x0_0x127_0}, to_apply=%region_0.1 | reduce-window | flops 4161536 | bytes 262148 | tf_op jit(solution)/shard_map/reduce-window
  19.8 0.1 slice.52
  19.9 0.1 copy.32
  20.1 0.1 copy.33
  20.2 0.0 collective-permute-done
  20.2 0.1 fusion.38
  20.2 0.0 collective-permute-done.1
  20.2 5.9 %fusion.18 = bf16[2048,256]{1,0:T(8,128)(2,1)} fusion(f32[2,256]{1,0:T(2,128)S(1)} %collective-permute-done.1, f32[2048,256]{1,0:T(8,128)} %copy-done.4, bf16[2048,256]{1,0:T(8,128)(2,1)} %param.16, f32[256]{0:T(256)S(1)} %bitcast.111, f32[256]{0:T(256)S(1)} %bitcast.112, f32[256]{0:T(256)S(1)} %bitcast.110, pred[2048]{0:T(1024)(128)(4,1)S(1)} %convert_compare_fusion, ...), kind=kLoop, calls=%fused_computation.29 | loop fusion | flops 6815744 | bytes 4205568 | tf_op jit(solution)/shard_map/convert_element_type | solution.py:47
  26.1 4.3 %all-to-all-start = ((bf16[4,512,256]{2,1,0:T(8,128)(2,1)}), bf16[4,512,256]{2,1,0:T(8,128)(2,1)S(1)}, u32[]{:S(2)}, u32[]{:S(2)}) async-start(bf16[4,512,256]{2,1,0:T(8,128)(2,1)} %bitcast.104), calls=%async_computation | async-start | bytes 2097152 | tf_op jit(solution)/shard_map/all_to_all | solution.py:48
  30.4 0.6 broadcast_multiply_fusion
  31.0 0.8 copy.29
  31.9 0.8 mul.115
  32.6 0.1 broadcast_add_fusion
  32.7 0.7 fusion.35
  33.5 0.7 compare_select_fusion
  34.2 11.6 %all-to-all-done = bf16[4,512,256]{2,1,0:T(8,128)(2,1)S(1)} async-done(((bf16[4,512,256]{2,1,0:T(8,128)(2,1)}), bf16[4,512,256]{2,1,0:T(8,128)(2,1)S(1)}, u32[]{:S(2)}, u32[]{:S(2)}) %all-to-all-start) | async-done | bytes 1048608 | tf_op jit(solution)/shard_map/all_to_all | solution.py:48
  45.7 0.0 copy-start.6
  45.7 1.0 copy-done.6
  46.7 1.5 copy.28
  48.2 0.0 copy-start.9
  48.2 5.5 %multiply_reduce_fusion.1 = (f32[512]{0:T(512)S(1)}, f32[512,2048]{1,0:T(8,128)S(1)}) fusion(bf16[512,1024]{0,1:T(8,128)(2,1)S(1)} %bitcast.102, bf16[1024,2048]{1,0:T(8,128)(2,1)} %param.19, bf16[512,2048]{1,0:T(8,128)(2,1)} %param.13), kind=kOutput, calls=%fused_computation.17 | convolution fusion | flops 2151677440 | bytes 11536384 | tf_op jit(solution)/shard_map/dot_general | solution.py:49
  53.8 1.9 copy-done.2
  55.7 0.0 copy-done.9
  55.7 0.4 multiply_convert_fusion
  56.1 3.8 %broadcast_in_dim.46 = bf16[512,2,2048]{2,1,0:T(2,128)(2,1)} broadcast(bf16[512,2048]{1,0:T(8,128)(2,1)S(1)} %multiply_convert_fusion), dimensions={0,2} | broadcast | bytes 6291456 | tf_op jit(solution)/shard_map/broadcast_in_dim | solution.py:59
  59.9 7.2 %reshape.125 = bf16[1024,2048]{1,0:T(8,128)(2,1)} reshape(bf16[512,2,2048]{2,1,0:T(2,128)(2,1)} %broadcast_in_dim.46) | data formatting | bytes 8388608 | tf_op jit(solution)/shard_map/reshape | solution.py:59
  67.0 12.3 %scatter_custom_fusion = bf16[2048,2048]{1,0:T(8,128)(2,1)} fusion(s32[1024]{0:T(1024)S(1)} %bitcast.108, bf16[1024,2048]{1,0:T(8,128)(2,1)} %reshape.125, bf16[]{:T(256)} %constant.5.clone.1), kind=kCustom, calls=%fused_computation.18 | custom fusion | bytes 8389120 | tf_op jit(solution)/shard_map/scatter | solution.py:60
  79.3 104.0 %all_to_all.29 = bf16[32,1,64,2048]{3,2,1,0:T(8,128)(2,1)S(1)} all-to-all(bf16[32,1,64,2048]{3,2,1,0:T(8,128)(2,1)} %bitcast.101), channel_id=1, replica_groups=mesh['sp'=32,'tp'=4] {'sp'}, dimensions={0} | all-to-all | bytes 16777216 | tf_op jit(solution)/shard_map/all_to_all | solution.py:62
  183.4 0.0 copy-start.5
  183.4 3.2 copy-done.5
  186.6 0.0 copy-done.12
  186.6 6.0 %fusion = f32[32,64,512]{2,1,0:T(8,128)} fusion(bf16[32,1,64,2048]{3,2,1,0:T(8,128)(2,1)S(1)} %all_to_all.29, bf16[1,2048,512]{2,1,0:T(8,128)(2,1)S(1)} %copy-done.12), kind=kOutput, calls=%fused_computation.2 | convolution fusion | flops 4294967296 | bytes 14680064 | tf_op jit(solution)/shard_map/aend,edf->aenf/dot_general | solution.py:64
  192.6 0.0 copy-done
  192.6 14.8 %convert_bitcast_fusion = bf16[32,1,64,2048]{3,2,1,0:T(8,128)(2,1)} fusion(bf16[1,512,2048]{2,1,0:T(8,128)(2,1)S(1)} %copy-done, f32[32,64,512]{2,1,0:T(8,128)} %fusion, bf16[32,1,64,2048]{3,2,1,0:T(8,128)(2,1)} %copy-done.5, bf16[1,2048,512]{2,1,0:T(8,128)(2,1)} %param.23), kind=kOutput, calls=%fused_computation.7 | convolution fusion | flops 8600420352 | bytes 25165824 | tf_op jit(solution)/shard_map/aenf,efd->aend/dot_general | solution.py:66
  207.4 0.0 copy-start.11
  207.4 5.3 %all-to-all-start.2 = ((bf16[32,1,64,2048]{3,2,1,0:T(8,128)(2,1)}), bf16[32,1,64,2048]{3,2,1,0:T(8,128)(2,1)}, u32[]{:S(2)}, u32[]{:S(2)}) async-start(bf16[32,1,64,2048]{3,2,1,0:T(8,128)(2,1)} %convert_bitcast_fusion), calls=%async_computation.2 | async-start | bytes 16777216 | tf_op jit(solution)/shard_map/all_to_all | solution.py:69
  212.7 0.0 copy-done.11
  212.7 0.1 copy.35
  212.9 105.5 %all-to-all-done.2 = bf16[32,1,64,2048]{3,2,1,0:T(8,128)(2,1)} async-done(((bf16[32,1,64,2048]{3,2,1,0:T(8,128)(2,1)}), bf16[32,1,64,2048]{3,2,1,0:T(8,128)(2,1)}, u32[]{:S(2)}, u32[]{:S(2)}) %all-to-all-start.2) | async-done | bytes 8388640 | tf_op jit(solution)/shard_map/all_to_all | solution.py:69
  318.4 13.3 %gather_fusion = bf16[1024,2048]{1,0:T(8,128)(2,1)} fusion(bf16[2048,2048]{1,0:T(8,128)(2,1)} %bitcast.31, s32[1024]{0:T(1024)S(1)} %broadcast_clamp_fusion), kind=kCustom, calls=%fused_computation | custom fusion | bytes 8392704 | tf_op jit(solution)/shard_map/gather | solution.py:72
  331.7 9.7 %reshape.112 = f32[512,2,2048]{2,1,0:T(2,128)} reshape(bf16[1024,2048]{1,0:T(8,128)(2,1)} %gather_fusion) | data formatting | bytes 12582912 | tf_op jit(solution)/shard_map/convert_element_type | solution.py:72
  341.4 0.0 copy-start.3
  341.4 0.0 copy-start.1
  341.4 14.2 %multiply_reduce_fusion = f32[512,2048]{1,0:T(8,128)S(1)} fusion(f32[512,2,2048]{2,1,0:T(2,128)} %reshape.112, f32[512,2]{1,0:T(8,128)S(1)} %copy.35), kind=kLoop, calls=%fused_computation.6 | loop fusion | flops 3145728 | bytes 12587008 | tf_op jit(solution)/shard_map/reduce_sum | solution.py:73
  355.6 0.0 copy-done.3
  355.6 1.9 add_convert_fusion
  357.5 0.0 copy-done.1
  (10 shorter events, 0.1 us)
Async XLA Ops:
  0.0 192.6 %copy-start = (bf16[1,512,2048]{2,1,0:T(8,128)(2,1)S(1)}, bf16[1,512,2048]{2,1,0:T(8,128)(2,1)}, u32[]{:S(2)}) copy-start(bf16[1,512,2048]{2,1,0:T(8,128)(2,1)} %param.25) | copy-start | bytes 6291460
  0.0 9.7 %copy-start.7 = (s32[2048]{0:T(1024)S(1)}, s32[2048]{0:T(1024)}, u32[]{:S(2)}) copy-start(s32[2048]{0:T(1024)} %param.18) | copy-start | bytes 24580
  0.0 9.7 %copy-start.8 = (s32[512,2]{0,1:T(2,128)S(1)}, s32[512,2]{0,1:T(2,128)}, u32[]{:S(2)}) copy-start(s32[512,2]{0,1:T(2,128)} %param.21) | copy-start | bytes 12292
  0.0 10.8 %copy-start.10 = (bf16[3,256]{1,0:T(4,128)(2,1)S(1)}, bf16[3,256]{1,0:T(4,128)(2,1)}, u32[]{:S(2)}) copy-start(bf16[3,256]{1,0:T(4,128)(2,1)} %param.17) | copy-start | bytes 4612
  0.9 19.2 %collective-permute-start = (f32[2]{0:T(128)S(1)}, f32[2]{0:T(128)S(1)}, u32[]{:S(2)}, u32[]{:S(2)}) collective-permute-start(f32[2]{0:T(128)S(1)} %slice.46), channel_id=1, source_target_pairs={{0,4},{4,8},{8,12},{12,16},{16,20},{20,24},{24,28},{28,32},{32,36}... | collective-permute-start | bytes 32 | tf_op jit(solution)/shard_map/ppermute | solution.py:16
  4.0 1.3 copy-start.4
  5.3 14.9 %collective-permute-start.1 = (f32[2,256]{1,0:T(2,128)S(1)}, f32[2,256]{1,0:T(2,128)S(1)}, u32[]{:S(2)}, u32[]{:S(2)}) collective-permute-start(f32[2,256]{1,0:T(2,128)S(1)} %slice.49), channel_id=1, source_target_pairs={{0,4},{4,8},{8,12},{12,16},{16,20},{20,24},{24,28},{28,32},{32,36}... | collective-permute-start | bytes 6152 | tf_op jit(solution)/shard_map/ppermute | solution.py:16
  26.1 19.6 %all-to-all-start = ((bf16[4,512,256]{2,1,0:T(8,128)(2,1)}), bf16[4,512,256]{2,1,0:T(8,128)(2,1)S(1)}, u32[]{:S(2)}, u32[]{:S(2)}) async-start(bf16[4,512,256]{2,1,0:T(8,128)(2,1)} %bitcast.104), calls=%async_computation | async-start | bytes 2097152 | tf_op jit(solution)/shard_map/all_to_all | solution.py:48
  45.7 1.0 copy-start.6
  48.2 7.5 %copy-start.9 = (f32[2048]{0:T(1024)S(1)}, f32[2048]{0:T(1024)}, u32[]{:S(2)}) copy-start(f32[2048]{0:T(1024)} %param.20) | copy-start | bytes 24580
  53.7 1.9 copy-start.2
  79.3 107.2 %copy-start.12 = (bf16[1,2048,512]{2,1,0:T(8,128)(2,1)S(1)}, bf16[1,2048,512]{2,1,0:T(8,128)(2,1)}, u32[]{:S(2)}) copy-start(bf16[1,2048,512]{2,1,0:T(8,128)(2,1)} %param.24) | copy-start | bytes 6291460
  183.4 3.2 copy-start.5
  207.4 5.4 %copy-start.11 = (f32[512,2]{0,1:T(2,128)S(1)}, f32[512,2]{0,1:T(2,128)}, u32[]{:S(2)}) copy-start(f32[512,2]{0,1:T(2,128)} %param.22) | copy-start | bytes 12292
  207.4 111.0 %all-to-all-start.2 = ((bf16[32,1,64,2048]{3,2,1,0:T(8,128)(2,1)}), bf16[32,1,64,2048]{3,2,1,0:T(8,128)(2,1)}, u32[]{:S(2)}, u32[]{:S(2)}) async-start(bf16[32,1,64,2048]{3,2,1,0:T(8,128)(2,1)} %convert_bitcast_fusion), calls=%async_computation.2 | async-start | bytes 16777216 | tf_op jit(solution)/shard_map/all_to_all | solution.py:69
  341.4 14.2 %copy-start.3 = (f32[512,2048]{1,0:T(8,128)S(1)}, f32[512,2048]{1,0:T(8,128)}, u32[]{:S(2)}) copy-start(f32[512,2048]{1,0:T(8,128)} %copy-done.2) | copy-start | bytes 12582916
  341.4 16.1 %copy-start.1 = (bf16[1,512,2048]{2,1,0:T(8,128)(2,1)S(1)}, bf16[1,512,2048]{2,1,0:T(8,128)(2,1)}, u32[]{:S(2)}) copy-start(bf16[1,512,2048]{2,1,0:T(8,128)(2,1)} %param.25) | copy-start | bytes 6291460
where the time goes:
time: 358 us
  waiting for transfers between devices  117 us (33%)
  blocking collectives  104 us (29%)
  local copies, waits for them, and re-layouts  58.4 us (16%)
  other arithmetic  36.3 us (10%)
  matrix products  26.3 us (7%)
  starting transfers between devices  15.2 us (4%)
    all_to_all x1, waiting for transfers between devices, per_device(): lax.all_to_all(expert_out, 'sp', split_axis=0, concat_axis=0, tiled=True)  105 us
    all_to_all x1, blocking collectives, per_device(): lax.all_to_all(buffer, 'sp', split_axis=0, concat_axis=0, tiled=True)  104 us
    dot_general x1, matrix products, per_device(): jnp.einsum('aenf,efd->aend', act_rows, w_down, preferred_element_type=jnp...  14.8 us
    reduce_sum x1, other arithmetic, per_device(): expert_sum = jnp.sum(picked.reshape(-1, 2, model_width), axis=1)  14.2 us
    gather x1, local copies, waits for them, and re-layouts, per_device(): returned[slot_index].astype(jnp.float32)  13.3 us
    scatter x1, local copies, waits for them, and re-layouts, per_device(): jnp.zeros((EXPERTS * CAP, model_width), jnp.bfloat16).at[slot_index]  12.3 us
    all_to_all x1, waiting for transfers between devices, per_device(): lax.all_to_all(gated, 'tp', split_axis=0, concat_axis=1, tiled=True)  11.6 us
    convert_element_type x1, local copies, waits for them, and re-layouts, per_device(): returned[slot_index].astype(jnp.float32)  9.68 us
  transfers between devices with their start and end apart: 4, of which 2 were waited for; matrix products, arithmetic and copies ran while one was open for 5% of the time, Pallas kernels for 0%

commit v1 on v0

v1 whole, which is shorter than its diff:
```python
import jax
import jax.numpy as jnp
from jax import lax
from jax.sharding import PartitionSpec as P

EXPERTS = 32
CAP = 64
CHUNKS = 1

epsilon = 1e-06
f32 = jnp.float32
bf16 = jnp.bfloat16


def from_behind(x, axis, by):
    devices = lax.axis_size(axis)
    pairs = [(i, i + by) for i in range(devices) if 0 <= i + by < devices]
    return lax.ppermute(x, axis, pairs)


def exchange(x, axis):
    return lax.all_to_all(x, axis, split_axis=0, concat_axis=0, tiled=True)


def per_device(
    residual_in,
    conv_input,
    input_gate,
    output_gate,
    conv_taps,
    doc_ids,
    proj_weight,
    norm_gain,
    expert_ids,
    expert_weight,
    w_gate,
    w_up,
    w_down,
):
    width = residual_in.shape[1]
    tokens = residual_in.shape[0]
    length, channels = conv_input.shape
    rim = conv_taps.shape[0] - 1

    doc_float = doc_ids.astype(f32)
    tail = input_gate[-rim:].astype(f32) * conv_input[-rim:].astype(f32)
    packed = jnp.concatenate([tail, jnp.broadcast_to(doc_float[-rim:, None], (rim, 128))], axis=1)
    behind = from_behind(packed, "sp", 1)
    product = input_gate.astype(f32) * conv_input.astype(f32)
    padded_in = jnp.concatenate([behind[:, :channels], product], axis=0)
    padded_ids = jnp.concatenate([behind[:, channels], doc_float], axis=0)
    conv_sum = jnp.zeros(product.shape, f32)
    for offset in range(rim + 1):
        same_doc = padded_ids[offset : offset + length] == doc_float
        term = conv_taps[offset].astype(f32)[None, :] * padded_in[offset : offset + length]
        conv_sum = conv_sum + jnp.where(same_doc[:, None], term, 0.0)
    gated = (output_gate.astype(f32) * conv_sum).astype(bf16)
    regrouped = lax.all_to_all(gated, "tp", split_axis=0, concat_axis=1, tiled=True)

    experts = jnp.arange(EXPERTS, dtype=jnp.int32)
    named = expert_ids[:, :, None] == experts[None, None, :]
    chosen = jnp.any(named, axis=1)
    weight = jnp.sum(jnp.where(named, expert_weight[:, :, None], 0.0), axis=1)
    earlier = (jnp.arange(tokens)[:, None] > jnp.arange(tokens)[None, :]).astype(bf16)
    rank = jnp.dot(earlier, chosen.astype(bf16), preferred_element_type=f32)
    code = jnp.where(chosen, rank, -1.0)
    code_t = code.T

    mixed = jnp.dot(regrouped, proj_weight, preferred_element_type=f32)
    hidden = residual_in.astype(f32) + mixed
    scale_rows = lax.rsqrt(jnp.mean(hidden * hidden, axis=-1, keepdims=True) + epsilon)
    normed = (hidden * scale_rows * norm_gain[None, :]).astype(bf16)

    size = CAP // CHUNKS
    rows = EXPERTS * size
    sent = []
    for k in range(CHUNKS):
        ranks = (jnp.arange(size) + k * size).astype(f32)
        pick = (code_t[:, None, :] == ranks[None, :, None]).reshape(rows, tokens).astype(bf16)
        slots = jnp.dot(pick, normed, preferred_element_type=f32).astype(bf16)
        sent.append(exchange(slots.reshape(EXPERTS, size, width), "sp"))
    back = []
    for k in range(CHUNKS):
        slots = sent[k].reshape(rows, width)
        gate_val = jnp.dot(slots, w_gate[0], preferred_element_type=f32)
        up_val = jnp.dot(slots, w_up[0], preferred_element_type=f32)
        act_rows = (jax.nn.silu(gate_val) * up_val).astype(bf16)
        expert_out = jnp.dot(act_rows, w_down[0], preferred_element_type=f32).astype(bf16)
        back.append(exchange(expert_out.reshape(EXPERTS, size, width), "sp"))
    total = hidden
    for k in range(CHUNKS):
        ranks = (jnp.arange(size) + k * size).astype(f32)
        place = jnp.where(code[:, :, None] == ranks[None, None, :], weight[:, :, None], 0.0)
        place = place.reshape(tokens, rows).astype(bf16)
        total = total + jnp.dot(place, back[k].reshape(rows, width), preferred_element_type=f32)
    return total.astype(bf16)


def solution(mesh):
    return jax.shard_map(
        per_device,
        mesh=mesh,
        in_specs=(
            P(("sp", "tp"), None),
            P("sp", "tp"),
            P("sp", "tp"),
            P("sp", "tp"),
            P(None, "tp"),
            P("sp"),
            P(),
            P(),
            P(("sp", "tp"), None),
            P(("sp", "tp"), None),
            P("sp", None, None),
            P("sp", None, None),
            P("sp", None, None),
        ),
        out_specs=P(("sp", "tp"), None),
        check_vma=False,
    )
```

time: 358 us -> 286 us (0.80)
  local copies, waits for them, and re-layouts: 58.4 us -> 2.84 us
  other arithmetic: 36.3 us -> 8.46 us
  matrix products: 26.3 us -> 37.4 us
  starting transfers between devices: 15.2 us -> 11.5 us
    reduce_sum x2 -> x1, other arithmetic: 14.9 us -> 0.02 us  [per_device(): weight = jnp.sum(jnp.where(named, expert_weight[:, :, None], 0.0), axis=1)]
    gather x1 -> x0, local copies, waits for them, and re-layouts: 13.3 us -> none  [per_device(): returned[slot_index].astype(jnp.float32)]
    scatter x1 -> x0, local copies, waits for them, and re-layouts: 12.3 us -> none  [per_device(): jnp.zeros((EXPERTS * CAP, model_width), jnp.bfloat16).at[slot_index]]
    dot_general x3 -> x7, matrix products: 26.3 us -> 37.4 us  [the longest x1 9.88 us: per_device(): jnp.dot(place, back[k].reshape(rows, width), preferred_element_type=f32)]
    convert_element_type x1 -> x0, local copies, waits for them, and re-layouts: 9.68 us -> none  [per_device(): returned[slot_index].astype(jnp.float32)]
    another operation x3 -> x0, other arithmetic: 9.14 us -> none
    reshape x1 -> x0, local copies, waits for them, and re-layouts: 7.19 us -> none  [per_device(): source_rows = jnp.repeat(normed, 2, axis=0)]
    unnamed x28 -> x24, local copies, waits for them, and re-layouts: 7.74 us -> 1.02 us
  transfers between devices with their start and end apart: 4 -> 3, of which waited for: 2 -> 2; matrix products, arithmetic and copies ran while one was open for 5% -> 1% of each run, Pallas kernels for 0% -> 0%
where the time goes in v1:
time: 286 us; the launch traced here: 285 us
  waiting for transfers between devices  120 us (42%)
  blocking collectives  105 us (37%)
  matrix products  37.4 us (13%)
  starting transfers between devices  11.5 us (4%)
  other arithmetic  8.46 us (3%)
    all_to_all x1, waiting for transfers between devices, exchange(): return lax.all_to_all(x, axis, split_axis=0, concat_axis=0, tiled=True)  106 us
    all_to_all x1, blocking collectives, exchange(): return lax.all_to_all(x, axis, split_axis=0, concat_axis=0, tiled=True)  105 us
    all_to_all x1, waiting for transfers between devices, per_device(): lax.all_to_all(gated, 'tp', split_axis=0, concat_axis=1, tiled=True)  13.9 us
    dot_general x1, matrix products, per_device(): jnp.dot(place, back[k].reshape(rows, width), preferred_element_type=f32)  9.88 us
    dot_general x1, matrix products, per_device(): jnp.dot(act_rows, w_down[0], preferred_element_type=f32).astype(bf16)  6.73 us
    dot_general x1, matrix products, per_device(): mixed = jnp.dot(regrouped, proj_weight, preferred_element_type=f32)  5.8 us
  transfers between devices with their start and end apart: 3, of which 2 were waited for; matrix products, arithmetic and copies ran while one was open for 1% of the time, Pallas kernels for 0%

profile of v1, /device:TPU:0, one launch (start us, length us, event | category | flops | bytes accessed | tf_op | source)
XLA Modules:
  0.0 285.2 jit_solution(16955820489937835222)
XLA Ops:
  0.0 0.0 copy-start
  0.0 0.8 convert_element_type.70
  0.9 0.0 copy-start.5
  0.9 0.1 slice.48
  0.9 0.7 convert_multiply_fusion.1
  1.6 0.1 broadcast_in_dim.76
  1.7 0.0 copy-start.7
  1.7 0.0 copy-start.4
  1.7 1.4 collective-permute-start
  3.2 1.8 convert_multiply_fusion
  4.9 0.0 copy-done.5
  5.0 0.0 copy-done.7
  5.0 0.0 collective-permute-done
  5.0 0.1 slice_reduce_fusion
  5.1 0.1 fusion.22
  5.2 0.0 copy-done.4
  5.2 3.3 %fusion.7 = bf16[2048,256]{1,0:T(8,128)(2,1)} fusion(f32[2,256]{1,0:T(2,128)S(1)} %slice.52, f32[2048,256]{1,0:T(8,128)S(1)} %convert_multiply_fusion, bf16[2048,256]{1,0:T(8,128)(2,1)S(1)} %copy-done.4, f32[256]{0:T(256)S(1)} %bitcast.42, f32[256]{0:T(256)S(1)} %bitcast.43, f32[256]{0:T(256)S(1)} %bitcast.41, pred[2048]{0:T(1024)(128)(4,1)S(1)} %convert_compare_fusion, ...), kind=kLoop, calls=%fused_computation.18 | loop fusion | flops 6815744 | bytes 4205568 | tf_op jit(solution)/shard_map/convert_element_type | solution.py:57
  8.5 0.0 copy-start.6
  8.5 5.0 %all-to-all-start = ((bf16[4,512,256]{2,1,0:T(8,128)(2,1)}), bf16[4,512,256]{2,1,0:T(8,128)(2,1)S(1)}, u32[]{:S(2)}, u32[]{:S(2)}) async-start(bf16[4,512,256]{2,1,0:T(8,128)(2,1)} %bitcast.39), calls=%async_computation | async-start | bytes 2097152 | tf_op jit(solution)/shard_map/all_to_all | solution.py:58
  13.5 0.1 eq.69
  13.6 0.0 copy-done.6
  13.6 0.2 convolution_select_fusion
  13.9 1.6 bitcast_compare_fusion
  15.5 13.9 %all-to-all-done = bf16[4,512,256]{2,1,0:T(8,128)(2,1)S(1)} async-done(((bf16[4,512,256]{2,1,0:T(8,128)(2,1)}), bf16[4,512,256]{2,1,0:T(8,128)(2,1)S(1)}, u32[]{:S(2)}, u32[]{:S(2)}) %all-to-all-start) | async-done | bytes 1048608 | tf_op jit(solution)/shard_map/all_to_all | solution.py:58
  29.4 0.0 copy-start.2
  29.4 1.0 copy-done.2
  30.4 1.5 copy.24
  31.9 0.0 copy-start.3
  31.9 0.0 copy-start.11
  31.9 5.8 %multiply_reduce_fusion = (f32[512]{0:T(512)S(1)}, f32[512,2048]{1,0:T(8,128)S(1)}) fusion(bf16[512,1024]{0,1:T(8,128)(2,1)S(1)} %bitcast.37, bf16[1024,2048]{1,0:T(8,128)(2,1)} %param.19, bf16[512,2048]{1,0:T(8,128)(2,1)} %param.13), kind=kOutput, calls=%fused_computation.7 | convolution fusion | flops 2151677440 | bytes 11536384 | tf_op jit(solution)/shard_map/dot_general | solution.py:69
  37.7 0.0 copy-start.1
  37.7 0.0 copy-done.3
  37.7 0.0 copy-done.11
  37.8 5.1 %convolution_convert_fusion.1 = bf16[2048,2048]{1,0:T(8,128)(2,1)S(1)} fusion(pred[2048,512]{1,0:T(32,128)(4,1)S(1)} %copy-done.3, f32[512,2048]{1,0:T(8,128)S(1)} %get-tuple-element.11, f32[2048]{0:T(1024)S(1)} %copy-done.11, f32[512]{0:T(512)S(1)} %add_rsqrt_fusion), kind=kOutput, calls=%fused_computation.1 | convolution fusion | flops 4302307328 | bytes 13641728 | tf_op jit(solution)/shard_map/dot_general | solution.py:80
  42.8 0.0 copy-done.1
  42.8 0.0 copy-start.9
  42.9 105.1 %all_to_all.29 = bf16[32,64,2048]{2,1,0:T(8,128)(2,1)S(1)} all-to-all(bf16[32,64,2048]{2,1,0:T(8,128)(2,1)S(1)} %bitcast.34), channel_id=1, replica_groups=mesh['sp'=32,'tp'=4] {'sp'}, dimensions={0} | all-to-all | bytes 16777216 | tf_op jit(solution)/shard_map/all_to_all | solution.py:22
  147.9 0.0 copy-done.9
  147.9 0.0 copy-start.10
  147.9 4.5 %fusion.12 = f32[2048,512]{1,0:T(8,128)S(1)} fusion(bf16[2048,2048]{1,0:T(8,128)(2,1)S(1)} %bitcast.35, bf16[1,2048,512]{2,1,0:T(8,128)(2,1)S(1)} %copy-done.9), kind=kOutput, calls=%fused_computation.24 | convolution fusion | flops 4294967296 | bytes 14680064 | tf_op jit(solution)/shard_map/dot_general | solution.py:85
  152.4 0.0 copy-done.10
  152.4 5.2 %multiply_convert_fusion = bf16[2048,512]{1,0:T(8,128)(2,1)S(1)} fusion(f32[2048,512]{1,0:T(8,128)S(1)} %fusion.12, bf16[2048,2048]{1,0:T(8,128)(2,1)S(1)} %bitcast.36, bf16[1,2048,512]{2,1,0:T(8,128)(2,1)S(1)} %copy-done.10), kind=kOutput, calls=%fused_computation.5 | convolution fusion | flops 4301258752 | bytes 16777216 | tf_op jit(solution)/shard_map/dot_general | solution.py:86
  157.6 0.0 copy-done
  157.6 6.7 %convolution_convert_fusion = bf16[2048,2048]{1,0:T(8,128)(2,1)} fusion(bf16[2048,512]{1,0:T(8,128)(2,1)S(1)} %multiply_convert_fusion, bf16[1,512,2048]{2,1,0:T(8,128)(2,1)S(1)} %copy-done), kind=kOutput, calls=%fused_computation | convolution fusion | flops 4299161600 | bytes 12582912 | tf_op jit(solution)/shard_map/dot_general | solution.py:88
  164.4 0.0 copy-start.8
  164.4 5.1 %all-to-all-start.2 = ((bf16[32,64,2048]{2,1,0:T(8,128)(2,1)}), bf16[32,64,2048]{2,1,0:T(8,128)(2,1)}, u32[]{:S(2)}, u32[]{:S(2)}) async-start(bf16[32,64,2048]{2,1,0:T(8,128)(2,1)} %bitcast.33), calls=%async_computation.2 | async-start | bytes 16777216 | tf_op jit(solution)/shard_map/all_to_all | solution.py:22
  169.5 0.0 copy-done.8
  169.5 105.8 %all-to-all-done.2 = bf16[32,64,2048]{2,1,0:T(8,128)(2,1)} async-done(((bf16[32,64,2048]{2,1,0:T(8,128)(2,1)}), bf16[32,64,2048]{2,1,0:T(8,128)(2,1)}, u32[]{:S(2)}, u32[]{:S(2)}) %all-to-all-start.2) | async-done | bytes 8388640 | tf_op jit(solution)/shard_map/all_to_all | solution.py:22
  275.4 9.9 %fusion = bf16[512,2048]{1,0:T(8,128)(2,1)} fusion(f32[512,2048]{1,0:T(8,128)} %copy-done.1, bf16[32,64,2048]{2,1,0:T(8,128)(2,1)} %all-to-all-done.2, bf16[512,32]{0,1:T(8,128)(2,1)S(1)} %select_reduce_fusion, f32[512,32]{0,1:T(8,128)S(1)} %convolution_select_fusion, f32[64]{0:T(128)S(1)} %iota_convert_fusion), kind=kOutput, calls=%fused_computation.3 | convolution fusion | flops 4299161600 | bytes 14778624 | tf_op jit(solution)/shard_map/dot_general | solution.py:95
  (9 shorter events, 0.1 us)
Async XLA Ops:
  0.0 157.6 %copy-start = (bf16[1,512,2048]{2,1,0:T(8,128)(2,1)S(1)}, bf16[1,512,2048]{2,1,0:T(8,128)(2,1)}, u32[]{:S(2)}) copy-start(bf16[1,512,2048]{2,1,0:T(8,128)(2,1)} %param.25) | copy-start | bytes 6291460
  0.9 4.1 %copy-start.5 = (s32[2048]{0:T(1024)S(1)}, s32[2048]{0:T(1024)}, u32[]{:S(2)}) copy-start(s32[2048]{0:T(1024)} %param.18) | copy-start | bytes 24580
  1.7 3.2 %copy-start.7 = (bf16[3,256]{1,0:T(4,128)(2,1)S(1)}, bf16[3,256]{1,0:T(4,128)(2,1)}, u32[]{:S(2)}) copy-start(bf16[3,256]{1,0:T(4,128)(2,1)} %param.17) | copy-start | bytes 4612
  1.7 3.5 %copy-start.4 = (bf16[2048,256]{1,0:T(8,128)(2,1)S(1)}, bf16[2048,256]{1,0:T(8,128)(2,1)}, u32[]{:S(2)}) copy-start(bf16[2048,256]{1,0:T(8,128)(2,1)} %param.16) | copy-start | bytes 3145732
  1.7 3.3 %collective-permute-start = (f32[2,384]{1,0:T(2,128)S(1)}, f32[2,384]{1,0:T(2,128)S(1)}, u32[]{:S(2)}, u32[]{:S(2)}) collective-permute-start(f32[2,384]{1,0:T(2,128)S(1)} %pad_maximum_fusion.2), channel_id=1, source_target_pairs={{0,4},{4,8},{8,12},{12,16},{16,20},{20,24},{24,28},{28,32},{32,36}... | collective-permute-start | bytes 9224 | tf_op jit(solution)/shard_map/ppermute | solution.py:18
  8.5 5.1 %copy-start.6 = (s32[512,2]{0,1:T(2,128)S(1)}, s32[512,2]{0,1:T(2,128)}, u32[]{:S(2)}) copy-start(s32[512,2]{0,1:T(2,128)} %param.21) | copy-start | bytes 12292
  8.5 20.9 %all-to-all-start = ((bf16[4,512,256]{2,1,0:T(8,128)(2,1)}), bf16[4,512,256]{2,1,0:T(8,128)(2,1)S(1)}, u32[]{:S(2)}, u32[]{:S(2)}) async-start(bf16[4,512,256]{2,1,0:T(8,128)(2,1)} %bitcast.39), calls=%async_computation | async-start | bytes 2097152 | tf_op jit(solution)/shard_map/all_to_all | solution.py:58
  29.4 1.0 copy-start.2
  31.9 5.8 %copy-start.3 = (pred[2048,512]{1,0:T(32,128)(4,1)S(1)}, pred[2048,512]{1,0:T(32,128)(4,1)}, u32[]{:S(2)}) copy-start(pred[2048,512]{1,0:T(32,128)(4,1)} %bitcast_compare_fusion) | copy-start | bytes 3145732
  31.9 5.8 %copy-start.11 = (f32[2048]{0:T(1024)S(1)}, f32[2048]{0:T(1024)}, u32[]{:S(2)}) copy-start(f32[2048]{0:T(1024)} %param.20) | copy-start | bytes 24580
  37.7 5.1 %copy-start.1 = (f32[512,2048]{1,0:T(8,128)}, f32[512,2048]{1,0:T(8,128)S(1)}, u32[]{:S(2)}) copy-start(f32[512,2048]{1,0:T(8,128)S(1)} %get-tuple-element.11) | copy-start | bytes 12582916
  42.8 105.1 %copy-start.9 = (bf16[1,2048,512]{2,1,0:T(8,128)(2,1)S(1)}, bf16[1,2048,512]{2,1,0:T(8,128)(2,1)}, u32[]{:S(2)}) copy-start(bf16[1,2048,512]{2,1,0:T(8,128)(2,1)} %param.23) | copy-start | bytes 6291460
  147.9 4.5 %copy-start.10 = (bf16[1,2048,512]{2,1,0:T(8,128)(2,1)S(1)}, bf16[1,2048,512]{2,1,0:T(8,128)(2,1)}, u32[]{:S(2)}) copy-start(bf16[1,2048,512]{2,1,0:T(8,128)(2,1)} %param.24) | copy-start | bytes 6291460
  164.4 5.1 %copy-start.8 = (f32[512,2]{0,1:T(2,128)S(1)}, f32[512,2]{0,1:T(2,128)}, u32[]{:S(2)}) copy-start(f32[512,2]{0,1:T(2,128)} %param.22) | copy-start | bytes 12292
  164.4 111.0 %all-to-all-start.2 = ((bf16[32,64,2048]{2,1,0:T(8,128)(2,1)}), bf16[32,64,2048]{2,1,0:T(8,128)(2,1)}, u32[]{:S(2)}, u32[]{:S(2)}) async-start(bf16[32,64,2048]{2,1,0:T(8,128)(2,1)} %bitcast.33), calls=%async_computation.2 | async-start | bytes 16777216 | tf_op jit(solution)/shard_map/all_to_all | solution.py:22
